TPU v7x, 512 devices: a whole 4x8x8 slice. The times are simulated.
512 devices in a mesh: sp: 64 (over z, y), fs: 4 (over x), tp: 2 (over core).
Axes of the slice: x: 4, y: 8, z: 8, core: 2. Of those that a mesh axis runs over, the one named last changes fastest.
Arguments:
- tokens: bfloat16 [4, 16384, 1024], P('fs', 'sp', 'tp'), may hold values from -6 to 6
- w_inner: bfloat16 [1024, 2048], P('sp', 'tp'), may hold values from -0.1875 to 0.1875
- w_gate: bfloat16 [1024, 2048], P('sp', 'tp'), may hold values from -0.1875 to 0.1875
- w_write: bfloat16 [1024, 512], P('sp', 'tp'), may hold values from -0.1875 to 0.1875
- w_read: bfloat16 [1024, 512], P('sp', 'tp'), may hold values from -0.1875 to 0.1875
- w_pool_in: bfloat16 [1024, 1024], P('sp', 'tp'), may hold values from -0.1875 to 0.1875
- w_step: bfloat16 [1024, 2, 32], replicated, may hold values from -0.1875 to 0.1875
- conv_inner: bfloat16 [5, 2048], replicated, may hold values from -2.5 to 2.5
- conv_cross: bfloat16 [5, 2, 512], replicated, may hold values from -2.5 to 2.5
- rate_log: float32 [2, 32], replicated, may hold values from -20 to -3
- decay_extra: float32 [4, 16384, 2, 32], P('fs', 'sp', None, 'tp'), may hold values from -1 to 0
- norm_gain: float32 [2048], replicated, may hold values from 0.1 to 1.9
- pool_mix: bfloat16 [4, 256, 256], replicated, may hold values from -0.375 to 0.375
- pool_gain: float32 [1024], replicated, may hold values from 0.1 to 1.9
- w_out_inner: bfloat16 [2048, 1024], P('tp', 'fs'), may hold values from -0.109375 to 0.109375
- w_out_pool: bfloat16 [1024, 1024], P('tp', 'fs'), may hold values from -0.109375 to 0.109375
Outputs:
- layer_out: bfloat16 [4, 16384, 1024], P('fs', ('sp', 'tp'))
All inputs are finite; a program needn't handle non-finite values.
Results may differ from a plain program's by a relative error of at most 0.0075.
Values may be sent and summed in bfloat16 or wider, within the bound.
A program may use at most 128 MiB of HBM per device.

v0:
```python
import jax
import jax.numpy as jnp
from jax import lax
from jax.sharding import Mesh
from jax.sharding import PartitionSpec as P

HEAD_DIM = 64
STATE = 128
POOL_DIM = 256
POOL_GROUPS = 4
CONV = 5
BLOCK = 128
GRID_W = 32
SP = ("sp_0", "sp_1")
SP_TP = ("sp_0", "sp_1", "tp")
EPSILON = 1e-05


def with_halo(block, sides, width):
    for axis, dim in sides:
        count = lax.axis_size(axis)
        forward = [(i, i + 1) for i in range(count - 1)]
        backward = [(target, source) for source, target in forward]
        low = lax.ppermute(
            lax.slice_in_dim(block, block.shape[dim] - width, None, axis=dim), axis, forward
        )
        high = lax.ppermute(lax.slice_in_dim(block, 0, width, axis=dim), axis, backward)
        block = jnp.concatenate([low, block, high], axis=dim)
    return block


def sent_together(arrays, axis, dim, along):
    ends, at = ([], 0)
    for a in arrays[:-1]:
        at += a.shape[along]
        ends.append(at)
    both = jnp.concatenate(arrays, axis=along)
    return tuple(jnp.split(lax.all_gather(both, axis, axis=dim, tiled=True), ends, axis=along))


def sent_to_all(value, axis):
    devices = lax.axis_size(axis)
    return lax.all_to_all(
        jnp.broadcast_to(value[None], (devices, *value.shape)), axis, 0, 0, tiled=True
    )


def in_order(pieces, dim):
    pieces = jnp.moveaxis(pieces, 0, dim)
    lengths = pieces.shape
    return pieces.reshape(*lengths[:dim], lengths[dim] * lengths[dim + 1], *lengths[dim + 2 :])


def gather_directly(value, axis, dim):
    pieces = sent_to_all(value, axis)
    return in_order(pieces, dim)


def nothing_yet(value, identity):
    return jax.tree.map(
        lambda part, zero: jnp.zeros_like(part) + jnp.asarray(zero, part.dtype), value, identity
    )


def prefix_by_axis(value, axes, combine, identity, reverse):
    before = start = nothing_yet(value, identity)
    subtotal = value
    for axis in reversed(axes):
        devices, mine = (lax.axis_size(axis), lax.axis_index(axis))
        pieces = jax.tree.map(
            lambda part, kind: lax.all_gather(part.astype(kind), axis),
            subtotal,
            jax.tree.map(lambda a: jnp.bfloat16 if a.dtype == jnp.float32 else a.dtype, value),
        )
        inside, subtotal = (start, start)
        for k in reversed(range(devices)) if reverse else range(devices):
            passed = k > mine if reverse else k < mine
            subtotal = combine(
                subtotal, jax.tree.map(lambda part, own: part[k].astype(own.dtype), pieces, value)
            )
            inside = jax.tree.map(lambda new, old: jnp.where(passed, new, old), subtotal, inside)
        before = combine(inside, before)
    return before


def cut_along(value, dim, devices):
    before, after = (value.shape[:dim], value.shape[dim + 1 :])
    return jnp.moveaxis(value.reshape(*before, devices, -1, *after), dim, 0)


def sum_at_owner(value, axis, dim):
    pieces = cut_along(value, dim, lax.axis_size(axis))
    arrived = lax.all_to_all(pieces, axis, split_axis=0, concat_axis=0, tiled=True)
    return arrived.astype(jnp.float32).sum(axis=0)


def merge_states(earlier, later):
    return (earlier[0] + later[0], earlier[1] * jnp.exp(later[0])[:, None, None] + later[1])


def local_summary(values, decays, writer_rows, read_rows, per_group):
    tokens_here, heads_here, head_width = values.shape
    groups_here = writer_rows.shape[1]
    blocks = tokens_here // BLOCK
    block_values = values.reshape(blocks, BLOCK, groups_here, per_group, head_width)
    cumulative = jnp.cumsum(
        jnp.transpose(decays.reshape(blocks, BLOCK, heads_here), (0, 2, 1)), axis=2
    )
    cumulative = cumulative.reshape(blocks, groups_here, per_group, BLOCK)
    writes_group = writer_rows.reshape(blocks, BLOCK, groups_here, STATE)
    reads_group = read_rows.reshape(blocks, BLOCK, groups_here, STATE)
    lower_mask = jnp.tril(jnp.ones((BLOCK, BLOCK), dtype=bool))
    segment_log = cumulative[..., :, None] - cumulative[..., None, :]
    weights = jnp.exp(jnp.where(lower_mask, segment_log, -jnp.inf))
    scores = jnp.einsum("bign,bjgn->bgij", reads_group, writes_group)
    inside = jnp.einsum("bgrij,bjgrp->bigrp", scores[:, :, None] * weights, block_values)
    tail_decay = jnp.exp(cumulative[..., -1:] - cumulative)
    block_states = jnp.einsum("bjgn,bgrj,bjgrp->bgrpn", writes_group, tail_decay, block_values)
    block_decay = cumulative[..., -1]
    block_ends = jnp.cumsum(block_decay, axis=0)
    starts = block_ends - block_decay
    order = jnp.arange(blocks, dtype=jnp.int32)
    earlier_mask = (order[:, None] > order[None, :])[:, :, None, None]
    link_decay = jnp.exp(jnp.where(earlier_mask, starts[:, None] - block_ends[None], -jnp.inf))
    entering = jnp.einsum("bcgr,cgrpn->bgrpn", link_decay, block_states)
    device_decay = block_ends[-1]
    summary = jnp.einsum("cgr,cgrpn->grpn", jnp.exp(device_decay[None] - block_ends), block_states)
    parts = (inside, cumulative, starts, entering, reads_group)
    return (
        parts,
        (device_decay.reshape(heads_here), summary.reshape(heads_here, head_width, STATE)),
    )


def finish(parts, incoming):
    inside, cumulative, starts, entering, reads_group = parts
    blocks, groups_here, per_group, block_len = cumulative.shape
    arriving = incoming[1].reshape(
        groups_here, per_group, incoming[1].shape[1], incoming[1].shape[2]
    )
    entering = entering + jnp.exp(starts)[..., None, None] * arriving[None]
    carried = jnp.einsum("bign,bgrpn->bigrp", reads_group, entering)
    carried = carried * jnp.transpose(jnp.exp(cumulative), (0, 3, 1, 2))[..., None]
    outcome = inside + carried
    return outcome.reshape(blocks * block_len, groups_here * per_group, outcome.shape[4])


def pool_local(pool_in, pool_mix, pool_gain, tp_rank, position, devices):
    reach_rows = 2 ** (POOL_GROUPS - 1)
    tokens_here = pool_in.shape[0]
    channels = pool_in.shape[1]
    groups_here = channels // POOL_DIM
    grid_rows = tokens_here // GRID_W
    all_rows = grid_rows * devices
    framed = with_halo(pool_in, ((SP, 0),), reach_rows * GRID_W)
    framed = framed.astype(jnp.float32).reshape(
        grid_rows + 2 * reach_rows, GRID_W, groups_here, POOL_DIM
    )
    row_running = jnp.cumsum(jnp.pad(framed, ((1, 0), (0, 0), (0, 0), (0, 0))), axis=0)
    row_index = position * grid_rows + jnp.arange(grid_rows, dtype=jnp.int32)
    col_index = jnp.arange(GRID_W, dtype=jnp.int32)
    mix_local = lax.dynamic_slice_in_dim(pool_mix, tp_rank * groups_here, groups_here, 0)
    gain_local = lax.dynamic_slice_in_dim(pool_gain, tp_rank * channels, channels, 0)
    results = []
    for slot_index in range(groups_here):
        group_index = tp_rank * groups_here + slot_index
        window = jnp.left_shift(jnp.int32(2), group_index)
        half_window = window // 2
        row_band = row_running[:, :, slot_index]
        box_sum = lax.dynamic_slice_in_dim(
            row_band, reach_rows - half_window + window, grid_rows, 0
        ) - lax.dynamic_slice_in_dim(row_band, reach_rows - half_window, grid_rows, 0)
        col_running = jnp.cumsum(
            jnp.pad(box_sum, ((0, 0), (reach_rows + 1, reach_rows), (0, 0))), axis=1
        )
        box_sum = lax.dynamic_slice_in_dim(
            col_running, reach_rows - half_window + window, GRID_W, 1
        ) - lax.dynamic_slice_in_dim(col_running, reach_rows - half_window, GRID_W, 1)
        row_counts = (
            jnp.clip(row_index - half_window + window, 0, all_rows)
            - jnp.clip(row_index - half_window, 0, all_rows)
        ).astype(jnp.float32)
        col_counts = (
            jnp.clip(col_index - half_window + window, 0, GRID_W)
            - jnp.clip(col_index - half_window, 0, GRID_W)
        ).astype(jnp.float32)
        average = box_sum / (row_counts[:, None, None] * col_counts[None, :, None])
        own_values = framed[reach_rows : reach_rows + grid_rows, :, slot_index]
        offsets = (average - own_values).astype(jnp.bfloat16).reshape(tokens_here, POOL_DIM)
        mixed_rows = jnp.dot(offsets, mix_local[slot_index], preferred_element_type=jnp.float32)
        gain_part = gain_local[slot_index * POOL_DIM : (slot_index + 1) * POOL_DIM]
        results.append((mixed_rows * gain_part).astype(jnp.bfloat16))
    return jnp.concatenate(results, axis=1)


def body(
    tokens,
    w_inner,
    w_gate,
    w_write,
    w_read,
    w_pool_in,
    w_step,
    conv_inner,
    conv_cross,
    rate_log,
    decay_extra,
    norm_gain,
    pool_mix,
    pool_gain,
    w_out_inner,
    w_out_pool,
):
    tp_rank = lax.axis_index("tp")
    out_weights = sent_together((w_out_inner, w_out_pool), "fs", 1, 0)
    whole_rows = gather_directly(tokens[0], "tp", 1)
    tokens_here = whole_rows.shape[0]
    inner_here = w_inner.shape[1]
    cross_here = w_write.shape[1]
    heads_here = inner_here // HEAD_DIM
    groups_here = cross_here // STATE
    per_group = heads_here // groups_here
    stacked = jnp.concatenate([w_inner, w_write, w_read, w_gate, w_pool_in], axis=1)
    projected = jnp.dot(
        whole_rows,
        lax.all_gather(stacked, SP, axis=0, tiled=True),
        preferred_element_type=jnp.float32,
    )
    projected = projected.astype(jnp.bfloat16)
    stream_cols = inner_here + 2 * cross_here
    streams = projected[:, :stream_cols]
    gate_in = projected[:, stream_cols : stream_cols + inner_here]
    pool_in = projected[:, stream_cols + inner_here :]
    rim_width = CONV // 2
    framed = with_halo(streams, ((SP, 0),), rim_width).astype(jnp.float32)
    conv_taps = jnp.concatenate(
        [
            lax.dynamic_slice_in_dim(conv_inner, tp_rank * inner_here, inner_here, 1),
            lax.dynamic_slice_in_dim(conv_cross[:, 0], tp_rank * cross_here, cross_here, 1),
            lax.dynamic_slice_in_dim(conv_cross[:, 1], tp_rank * cross_here, cross_here, 1),
        ],
        axis=1,
    ).astype(jnp.float32)
    running = jnp.zeros((tokens_here, stream_cols), jnp.float32)
    for offset in range(CONV):
        running = running + framed[offset : offset + tokens_here] * conv_taps[offset]
    activated = jax.nn.silu(running)
    values = activated[:, :inner_here].reshape(tokens_here, heads_here, HEAD_DIM)
    writer_rows = activated[:, inner_here : inner_here + cross_here].reshape(
        tokens_here, groups_here, STATE
    )
    read_rows = activated[:, inner_here + cross_here :].reshape(tokens_here, groups_here, STATE)
    step_weights = lax.dynamic_slice_in_dim(w_step, tp_rank * heads_here, heads_here, 2)
    raw_step = jnp.dot(
        whole_rows,
        step_weights.reshape(step_weights.shape[0], 2 * heads_here),
        preferred_element_type=jnp.float32,
    ).reshape(tokens_here, 2, heads_here)
    step_size = jax.nn.softplus(raw_step)
    decay_rates = jnp.exp(lax.dynamic_slice_in_dim(rate_log, tp_rank * heads_here, heads_here, 1))
    log_decay = -step_size * decay_rates[None] + decay_extra[0]
    ahead_parts, ahead_summary = local_summary(
        values * step_size[:, 0, :, None], log_decay[:, 0], writer_rows, read_rows, per_group
    )
    behind_parts, behind_summary = local_summary(
        (values * step_size[:, 1, :, None])[::-1],
        log_decay[::-1, 1],
        writer_rows[::-1],
        read_rows[::-1],
        per_group,
    )
    blank_state = (jnp.zeros_like(ahead_summary[0]), jnp.zeros_like(ahead_summary[1]))
    ahead_in = prefix_by_axis(ahead_summary, SP, merge_states, blank_state, False)
    behind_in = prefix_by_axis(behind_summary, SP, merge_states, blank_state, True)
    pooled = pool_local(
        pool_in, pool_mix, pool_gain, tp_rank, lax.axis_index(SP), lax.axis_size(SP)
    )
    mixed_sum = finish(ahead_parts, ahead_in) + finish(behind_parts, behind_in)[::-1]
    gated_out = mixed_sum * jax.nn.silu(gate_in.astype(jnp.float32)).reshape(
        tokens_here, heads_here, HEAD_DIM
    )
    rms_scale = lax.rsqrt(jnp.mean(gated_out * gated_out, axis=2, keepdims=True) + EPSILON)
    gain_local = lax.dynamic_slice_in_dim(norm_gain, tp_rank * inner_here, inner_here, 0).reshape(
        heads_here, HEAD_DIM
    )
    mixer_out = (
        (gated_out * rms_scale * gain_local).reshape(tokens_here, inner_here).astype(jnp.bfloat16)
    )
    inner_weights, pool_weights = out_weights
    summed = sum_at_owner(
        (
            jnp.dot(mixer_out, inner_weights, preferred_element_type=jnp.float32)
            + jnp.dot(pooled, pool_weights, preferred_element_type=jnp.float32)
        ).astype(jnp.bfloat16),
        "tp",
        0,
    )
    return summed.astype(jnp.bfloat16)[None]


def solution(mesh):
    finer = Mesh(
        mesh.devices.reshape(8, 8, mesh.shape["fs"], mesh.shape["tp"]), ("sp_0", "sp_1", "fs", "tp")
    )
    in_specs = (
        P("fs", SP, "tp"),
        P(SP, "tp"),
        P(SP, "tp"),
        P(SP, "tp"),
        P(SP, "tp"),
        P(SP, "tp"),
        P(),
        P(),
        P(),
        P(),
        P("fs", SP, None, "tp"),
        P(),
        P(),
        P(),
        P("tp", "fs"),
        P("tp", "fs"),
    )
    out_specs = P("fs", SP_TP, None)
    return jax.shard_map(body, mesh=finer, in_specs=in_specs, out_specs=out_specs, check_vma=False)
```

profile of v0, /device:TPU:1, one launch (start us, length us, event | category | flops | bytes accessed | tf_op | source)
XLA Modules:
  0.0 369.2 jit_solution(7352323665303950627)
XLA Ops:
  6.5 0.8 constant_dynamic-update-slice_fusion.4
  7.4 0.7 constant_dynamic-update-slice_fusion.3
  8.1 0.7 constant_dynamic-update-slice_fusion.2
  8.8 0.8 constant_dynamic-update-slice_fusion.1
  9.5 0.7 constant_dynamic-update-slice_fusion
  10.9 1.1 copy.59
  12.0 0.8 broadcast_in_dim.44
  12.9 10.3 %all-to-all-start = ((bf16[2,256,512]{1,2,0:T(8,128)(2,1)}), bf16[2,256,512]{1,2,0:T(8,128)(2,1)S(1)}, u32[]{:S(2)}, u32[]{:S(2)}) async-start(bf16[2,256,512]{1,2,0:T(8,128)(2,1)} %broadcast_in_dim.44), calls=%async_computation | async-start | bytes 1048576 | tf_op jit(solution)/shard_map/all_to_all | solution.py:43
  23.3 1.3 all-to-all-done
  24.9 1.2 reduce_window_sum.67
  27.1 78.8 %all-gather.11.cloned.1.call-done = bf16[1024,3072]{1,0:T(8,128)(2,1)} async-done(((bf16[16,3072]{1,0:T(8,128)(2,1)}), bf16[1024,3072]{1,0:T(8,128)(2,1)}) %all-gather.11.cloned.1.call-update) | async-done | bytes 6291472 | tf_op jit(solution)/shard_map/all_gather | solution.py:226
  105.9 4.6 %fusion = bf16[256,3072]{1,0:T(8,128)(2,1)S(1)} fusion(bf16[1024,3072]{1,0:T(8,128)(2,1)} %all-gather.11.cloned.1.call-done, bf16[256,1024]{0,1:T(8,128)(2,1)S(1)} %bitcast.451), kind=kOutput, calls=%fused_computation.1 | convolution fusion | flops 1611399168 | bytes 8388608 | tf_op jit(solution)/shard_map/dot_general | solution.py:224
  110.6 1.3 collective-permute-start.1
  111.9 4.0 %collective-permute-start = (bf16[2,1536]{1,0:T(2,128)(2,1)S(1)}, bf16[2,1536]{1,0:T(2,128)(2,1)S(1)}, u32[]{:S(2)}, u32[]{:S(2)}) collective-permute-start(bf16[2,1536]{1,0:T(2,128)(2,1)S(1)} %get-tuple-element.94), channel_id=1, source_target_pairs={{0,8},{8,16},{16,24},{24,32},{32,40},{40,48},{48,56},{56,64},{64,7... | collective-permute-start | bytes 18440 | tf_op jit(solution)/shard_map/ppermute | solution.py:24
  116.9 1.1 divide_multiply_fusion
  119.1 1.5 broadcast_multiply_fusion.2
  120.9 0.7 fusion.63
  121.6 0.7 convert_element_type.916
  122.6 1.2 reduce_window_sum.70
  124.8 1.4 rev.15
  126.1 1.7 reshape.1089
  129.6 0.7 convert_element_type.986
  130.5 14.0 %all-gather = bf16[8,1,16]{2,1,0:T(2,128)(2,1)S(1)} all-gather(bf16[1,1,16]{2,1,0:T(2,128)(2,1)S(1)} %reshape.1178), channel_id=1, replica_groups=mesh['sp_0'=8,'sp_1'=8,'fs'=4,'tp'=2] {'sp_1'}, dimensions={0}, use_global_device_ids=true | all-gather | bytes 288 | tf_op jit(solution)/shard_map/all_gather | solution.py:71
  144.6 19.8 %all-gather.13.cloned.1.call-done = bf16[8,16,64,128]{3,2,1,0:T(8,128)(2,1)} async-done(((bf16[1,16,64,128]{3,2,1,0:T(8,128)(2,1)}), bf16[8,16,64,128]{3,2,1,0:T(8,128)(2,1)}) %all-gather.13.cloned.1.call-update) | async-done | bytes 2097168 | tf_op jit(solution)/shard_map/all_gather | solution.py:71
  164.5 2.7 add_convert_fusion.1
  167.4 11.4 %all-gather.2 = bf16[8,1,16]{2,1,0:T(2,128)(2,1)S(1)} all-gather(bf16[1,1,16]{2,1,0:T(2,128)(2,1)S(1)} %reshape.1182), channel_id=1, replica_groups=mesh['sp_0'=8,'sp_1'=8,'fs'=4,'tp'=2] {'sp_1'}, dimensions={0}, use_global_device_ids=true | all-gather | bytes 288 | tf_op jit(solution)/shard_map/all_gather | solution.py:71
  178.9 29.9 %all-gather.17.cloned.1.call-done = bf16[8,16,64,128]{3,2,1,0:T(8,128)(2,1)} async-done(((bf16[1,16,64,128]{3,2,1,0:T(8,128)(2,1)}), bf16[8,16,64,128]{3,2,1,0:T(8,128)(2,1)}) %all-gather.17.cloned.1.call-update) | async-done | bytes 2097168 | tf_op jit(solution)/shard_map/all_gather | solution.py:71
  208.8 2.7 add_convert_fusion
  211.7 1.0 pad_maximum_fusion
  221.8 13.7 %all-gather.3 = bf16[8,1,16]{2,1,0:T(2,128)(2,1)S(1)} all-gather(bf16[1,1,16]{2,1,0:T(2,128)(2,1)S(1)} %get-tuple-element.46), channel_id=1, replica_groups=mesh['sp_0'=8,'sp_1'=8,'fs'=4,'tp'=2] {'sp_0'}, dimensions={0}, use_global_device_ids=true | all-gather | bytes 288 | tf_op jit(solution)/shard_map/all_gather | solution.py:71
  235.5 12.3 %all-gather.1 = bf16[8,1,16]{2,1,0:T(2,128)(2,1)S(1)} all-gather(bf16[1,1,16]{2,1,0:T(2,128)(2,1)S(1)} %get-tuple-element.50), channel_id=1, replica_groups=mesh['sp_0'=8,'sp_1'=8,'fs'=4,'tp'=2] {'sp_0'}, dimensions={0}, use_global_device_ids=true | all-gather | bytes 288 | tf_op jit(solution)/shard_map/all_gather | solution.py:71
  268.7 1.3 convert_multiply_fusion
  270.0 1.0 slice.520
  271.0 1.3 collective-permute-start.3
  272.3 4.7 %collective-permute-start.2 = (bf16[256,512]{1,0:T(8,128)(2,1)S(1)}, bf16[256,512]{1,0:T(8,128)(2,1)}, u32[]{:S(2)}, u32[]{:S(2)}) collective-permute-start(bf16[256,512]{1,0:T(8,128)(2,1)S(1)} %slice.520), channel_id=1, source_target_pairs={{0,8},{8,16},{16,24},{24,32},{32,40},{40,48},{48,56},{56,64},{64,7... | collective-permute-start | bytes 786440 | tf_op jit(solution)/shard_map/ppermute | solution.py:24
  277.3 0.9 fusion.106
  278.5 0.9 fusion.103
  279.6 2.5 maximum_convert_fusion.1
  282.0 2.3 reshape.1139
  287.0 0.9 fusion.37
  287.9 1.9 slice_convert_fusion.15
  289.8 0.8 copy-done.4
  290.6 1.9 slice_convert_fusion.7
  292.7 1.8 fusion.242
  295.2 1.3 fusion.79
  296.6 0.9 fusion.32
  297.9 0.7 copy-done.26
  298.6 0.9 fusion.22
  299.5 1.8 copy.77
  301.4 2.1 reshape.1087
  303.7 1.8 fusion.241
  306.1 1.3 fusion.68
  307.5 0.9 fusion.31
  308.8 0.9 copy-done.6
  309.7 0.9 fusion.28
  310.6 1.8 copy.94
  312.4 3.0 reshape.1094
  315.5 2.3 rev.19
  317.7 1.6 multiply_reduce_fusion
  319.7 31.8 %all-gather.21.cloned.1.call-done = bf16[1536,1024]{1,0:T(8,128)(2,1)} async-done(((bf16[1536,256]{1,0:T(8,128)(2,1)}), bf16[1536,1024]{1,0:T(8,128)(2,1)}) %all-gather.21.cloned.1.call-update) | async-done | bytes 3145744 | tf_op jit(solution)/shard_map/all_gather | solution.py:38
  351.5 2.4 fusion.1
  353.9 1.8 fusion.35
  355.7 5.8 %all_to_all.10 = bf16[2,128,1024]{2,1,0:T(8,128)(2,1)S(1)} all-to-all(bf16[2,128,1024]{2,1,0:T(8,128)(2,1)S(1)} %bitcast.452), channel_id=1, replica_groups=mesh['sp_0'=8,'sp_1'=8,'fs'=4,'tp'=2] {'tp'}, dimensions={0} | all-to-all | bytes 1048576 | tf_op jit(solution)/shard_map/all_to_all | solution.py:93
  361.5 0.8 reduce_sum.22
  (341 shorter events, 43.3 us)
Async XLA Ops:
  6.5 280.2 %copy-start = (bf16[4,256,256]{2,1,0:T(8,128)(2,1)S(1)}, bf16[4,256,256]{2,1,0:T(8,128)(2,1)}, u32[]{:S(2)}) copy-start(bf16[4,256,256]{2,1,0:T(8,128)(2,1)} %param.28) | copy-start | bytes 1572868
  6.5 16.7 %copy-start.95 = (f32[2,32]{1,0:T(2,128)S(1)}, f32[2,32]{1,0:T(2,128)}, u32[]{:S(2)}) copy-start(f32[2,32]{1,0:T(2,128)} %param.25) | copy-start | bytes 772
  6.5 16.7 %copy-start.47 = (bf16[1024,2,32]{0,2,1:T(8,128)(2,1)S(1)}, bf16[1024,2,32]{0,2,1:T(8,128)(2,1)}, u32[]{:S(2)}) copy-start(bf16[1024,2,32]{0,2,1:T(8,128)(2,1)} %param.22) | copy-start | bytes 393220
  6.5 99.4 %all-gather.11.cloned.1.call-start = ((), (), s32[]{:S(2)}) async-start(), calls=%async_computation.2 | async-start | bytes 6389760 | tf_op jit(solution)/shard_map/all_gather | solution.py:226
  10.3 14.5 %copy-start.48 = (f32[1,256,2,16]{1,3,2,0:T(8,128)S(1)}, f32[1,256,2,16]{1,3,2,0:T(8,128)}, u32[]{:S(2)}) copy-start(f32[1,256,2,16]{1,3,2,0:T(8,128)} %param.26) | copy-start | bytes 98308
  12.0 14.8 %copy-start.41 = (bf16[5,2,512]{2,1,0:T(2,128)(2,1)S(1)}, bf16[5,2,512]{2,1,0:T(2,128)(2,1)}, u32[]{:S(2)}) copy-start(bf16[5,2,512]{2,1,0:T(2,128)(2,1)} %param.24) | copy-start | bytes 30724
  12.0 15.1 %copy-start.57 = (bf16[5,2048]{1,0:T(8,128)(2,1)S(1)}, bf16[5,2048]{1,0:T(8,128)(2,1)}, u32[]{:S(2)}) copy-start(bf16[5,2048]{1,0:T(8,128)(2,1)} %param.23) | copy-start | bytes 61444
  12.9 11.7 %all-to-all-start = ((bf16[2,256,512]{1,2,0:T(8,128)(2,1)}), bf16[2,256,512]{1,2,0:T(8,128)(2,1)S(1)}, u32[]{:S(2)}, u32[]{:S(2)}) async-start(bf16[2,256,512]{1,2,0:T(8,128)(2,1)} %broadcast_in_dim.44), calls=%async_computation | async-start | bytes 1048576 | tf_op jit(solution)/shard_map/all_to_all | solution.py:43
  23.2 141.3 %all-gather.13.cloned.1.call-start = ((), (), s32[]{:S(2)}) async-start(), calls=%async_computation.3 | async-start | bytes 2359296 | tf_op jit(solution)/shard_map/all_gather | solution.py:71
  26.2 84.4 %copy-start.43 = (f32[2,2,8]{2,1,0:T(2,128)}, f32[2,2,8]{2,1,0:T(2,128)S(1)}, u32[]{:S(2)}) copy-start(f32[2,2,8]{2,1,0:T(2,128)S(1)} %slice_reduce_fusion.1) | copy-start | bytes 388
  26.9 103.5 %copy-start.37 = (f32[2,2,8]{2,1,0:T(2,128)}, f32[2,2,8]{2,1,0:T(2,128)S(1)}, u32[]{:S(2)}) copy-start(f32[2,2,8]{2,1,0:T(2,128)S(1)} %fusion.249) | copy-start | bytes 388
  110.5 6.3 %copy-start.19 = (bf16[256,3072]{1,0:T(8,128)(2,1)}, bf16[256,3072]{1,0:T(8,128)(2,1)S(1)}, u32[]{:S(2)}) copy-start(bf16[256,3072]{1,0:T(8,128)(2,1)S(1)} %fusion) | copy-start | bytes 4718596
  110.6 5.5 %collective-permute-start.1 = (bf16[2,1536]{1,0:T(2,128)(2,1)S(1)}, bf16[2,1536]{1,0:T(2,128)(2,1)S(1)}, u32[]{:S(2)}, u32[]{:S(2)}) collective-permute-start(bf16[2,1536]{1,0:T(2,128)(2,1)S(1)} %get-tuple-element.95), channel_id=1, source_target_pairs={{8,0},{16,8},{24,16},{32,24},{40,32},{48,40},{56,48},{64,56},{72,6... | collective-permute-start | bytes 18440 | tf_op jit(solution)/shard_map/ppermute | solution.py:27
  111.9 4.8 %collective-permute-start = (bf16[2,1536]{1,0:T(2,128)(2,1)S(1)}, bf16[2,1536]{1,0:T(2,128)(2,1)S(1)}, u32[]{:S(2)}, u32[]{:S(2)}) collective-permute-start(bf16[2,1536]{1,0:T(2,128)(2,1)S(1)} %get-tuple-element.94), channel_id=1, source_target_pairs={{0,8},{8,16},{16,24},{24,32},{32,40},{40,48},{48,56},{56,64},{64,7... | collective-permute-start | bytes 18440 | tf_op jit(solution)/shard_map/ppermute | solution.py:24
  120.9 3.7 copy-start.24
  122.3 86.4 %all-gather.17.cloned.1.call-start = ((), (), s32[]{:S(2)}) async-start(), calls=%async_computation.5 | async-start | bytes 2359296 | tf_op jit(solution)/shard_map/all_gather | solution.py:71
  123.7 2.4 copy-start.31
  123.9 2.2 copy-start.45
  128.9 38.3 %copy-start.22 = (bf16[2,2,8,64,128]{4,3,2,1,0:T(8,128)(2,1)}, bf16[2,2,8,64,128]{4,3,2,1,0:T(8,128)(2,1)S(1)}, u32[]{:S(2)}) copy-start(bf16[2,2,8,64,128]{4,3,2,1,0:T(8,128)(2,1)S(1)} %fusion.43) | copy-start | bytes 1572868
  130.3 36.9 %copy-start.40 = (f32[2,2,8]{2,1,0:T(2,128)S(1)}, f32[2,2,8]{2,1,0:T(2,128)}, u32[]{:S(2)}) copy-start(f32[2,2,8]{2,1,0:T(2,128)} %copy-done.39) | copy-start | bytes 388
  130.4 162.1 %all-gather.15.cloned.1.call-start = ((), (), s32[]{:S(2)}) async-start(), calls=%async_computation.4 | async-start | bytes 2359296 | tf_op jit(solution)/shard_map/all_gather | solution.py:71
  167.2 44.4 %copy-start.20 = (bf16[1024,256]{1,0:T(8,128)(2,1)S(1)}, bf16[1024,256]{1,0:T(8,128)(2,1)}, u32[]{:S(2)}) copy-start(bf16[1024,256]{1,0:T(8,128)(2,1)} %param.30) | copy-start | bytes 1572868
  167.2 44.5 %copy-start.29 = (bf16[512,256]{1,0:T(8,128)(2,1)S(1)}, bf16[512,256]{1,0:T(8,128)(2,1)}, u32[]{:S(2)}) copy-start(bf16[512,256]{1,0:T(8,128)(2,1)} %param.31) | copy-start | bytes 786436
  167.2 136.4 %all-gather.19.cloned.1.call-start = ((), (), s32[]{:S(2)}) async-start(), calls=%async_computation.6 | async-start | bytes 2359296 | tf_op jit(solution)/shard_map/all_gather | solution.py:71
  211.5 3.1 copy-start.46
  211.5 3.8 %dynamic-slice-start = ((f32[2048]{0:T(1024)}, s32[]{:T(128)}), f32[1024]{0:T(1024)S(1)}, s32[]{:S(2)}) async-start(f32[2048]{0:T(1024)} %param.27, s32[]{:T(128)} %select_n.565), calls=%async_computation.8 | async-start | bytes 8704 | tf_op jit(solution)/shard_map/dynamic_slice | solution.py:283
  211.5 55.1 %copy-start.94 = (f32[1024]{0:T(1024)S(1)}, f32[1024]{0:T(1024)}, u32[]{:S(2)}) copy-start(f32[1024]{0:T(1024)} %param.29) | copy-start | bytes 12292
  211.6 139.9 %all-gather.21.cloned.1.call-start = ((), (), s32[]{:S(2)}) async-start(), calls=%async_computation.7 | async-start | bytes 3932160 | tf_op jit(solution)/shard_map/all_gather | solution.py:38
  271.0 8.4 %collective-permute-start.3 = (bf16[256,512]{1,0:T(8,128)(2,1)S(1)}, bf16[256,512]{1,0:T(8,128)(2,1)}, u32[]{:S(2)}, u32[]{:S(2)}) collective-permute-start(bf16[256,512]{1,0:T(8,128)(2,1)S(1)} %slice.520), channel_id=1, source_target_pairs={{8,0},{16,8},{24,16},{32,24},{40,32},{48,40},{56,48},{64,56},{72,6... | collective-permute-start | bytes 786440 | tf_op jit(solution)/shard_map/ppermute | solution.py:27
  272.3 7.3 %collective-permute-start.2 = (bf16[256,512]{1,0:T(8,128)(2,1)S(1)}, bf16[256,512]{1,0:T(8,128)(2,1)}, u32[]{:S(2)}, u32[]{:S(2)}) collective-permute-start(bf16[256,512]{1,0:T(8,128)(2,1)S(1)} %slice.520), channel_id=1, source_target_pairs={{0,8},{8,16},{16,24},{24,32},{32,40},{40,48},{48,56},{56,64},{64,7... | collective-permute-start | bytes 786440 | tf_op jit(solution)/shard_map/ppermute | solution.py:24
  287.9 2.7 copy-start.4
  292.5 2.2 copy-start.16
  292.5 2.3 copy-start.17
  292.6 2.5 copy-start.18
  292.6 2.5 copy-start.77
  292.6 2.4 copy-start.78
  292.6 2.4 copy-start.79
  292.6 2.4 copy-start.80
  292.6 2.4 copy-start.81
  292.6 2.4 copy-start.82
  292.6 2.4 copy-start.83
  292.6 2.4 copy-start.84
  292.6 2.4 copy-start.85
  292.7 2.4 copy-start.86
  292.7 2.4 copy-start.87
  292.7 2.4 copy-start.88
  292.7 2.4 copy-start.89
  292.7 2.4 copy-start.90
  292.7 2.4 copy-start.91
  292.7 2.4 copy-start.92
  292.7 2.4 copy-start.93
  303.4 2.1 copy-start.60
  303.4 2.1 copy-start.61
  303.4 2.1 copy-start.62
  303.5 2.1 copy-start.63
  303.5 2.1 copy-start.64
  303.5 2.1 copy-start.65
  303.5 2.1 copy-start.66
  303.5 2.1 copy-start.67
  303.7 2.1 copy-start.10
  303.7 2.3 copy-start.11
  303.7 2.4 copy-start.12
  351.5 2.4 copy-start.21
  353.9 8.4 %copy-start.1 = (bf16[4,256,256]{2,1,0:T(8,128)(2,1)S(1)}, bf16[4,256,256]{2,1,0:T(8,128)(2,1)}, u32[]{:S(2)}) copy-start(bf16[4,256,256]{2,1,0:T(8,128)(2,1)} %param.28) | copy-start | bytes 1572868
  (46 other events, 69.4 us)
Sparse Core Ops, SparseCore 0:
  11.0 94.8 all-gather.10
  122.5 41.9 all-gather.12
  166.5 42.1 all-gather.16
  210.7 42.7 all-gather.14
  255.5 47.0 all-gather.18
  304.5 46.9 all-gather.20
where the time goes:
time: 370 us; the launch traced here: 369 us
  waiting for transfers between devices  163 us (44%)
  local copies, waits for them, and re-layouts  62.2 us (17%)
  blocking collectives  57.1 us (15%)
  other arithmetic  32.1 us (9%)
  starting transfers between devices  21.7 us (6%)
  matrix products  18.1 us (5%)
  between operations  15.2 us (4%)
    all_gather x1, waiting for transfers between devices, body(): lax.all_gather(stacked, SP, axis=0, tiled=True)  78.8 us
    all_gather x4, blocking collectives, prefix_by_axis(): lax.all_gather(part.astype(kind), axis)  51.3 us
    all_gather x4, waiting for transfers between devices, prefix_by_axis(): lax.all_gather(part.astype(kind), axis)  49.8 us
    all_gather x1, waiting for transfers between devices, sent_together(): lax.all_gather(both, axis, axis=dim, tiled=True)  31.8 us
    exp x30, local copies, waits for them, and re-layouts, merge_states(): jnp.exp(later[0])[:, None, None]  19.4 us
    all_to_all x1, starting transfers between devices, sent_to_all(): lax.all_to_all(jnp.broadcast_to(value[None], (devices, *value.shape)), ax...  10.3 us
    ppermute x2, starting transfers between devices, with_halo(): lax.ppermute(lax.slice_in_dim(block, block.shape[dim] - width, None, axis...  8.68 us
    unnamed x205, local copies, waits for them, and re-layouts  7.85 us
  transfers between devices with their start and end apart: 11, of which 7 were waited for; matrix products, arithmetic and copies ran while one was open for 24% of the time, Pallas kernels for 0%

commit v1 on v0

--- a/solution.py
+++ b/solution.py
@@ -14,6 +14,13 @@
 SP = ("sp_0", "sp_1")
 SP_TP = ("sp_0", "sp_1", "tp")
 EPSILON = 1e-05
+
+
+def all_by_exchange(x, axis, dim):
+    devices = lax.axis_size(axis)
+    parts = jnp.stack([x for _ in range(devices)])
+    parts = lax.all_to_all(parts, axis, split_axis=0, concat_axis=0)
+    return jnp.concatenate(parts, axis=dim)
 
 
 def with_halo(block, sides, width):
@@ -222,9 +229,7 @@
     per_group = heads_here // groups_here
     stacked = jnp.concatenate([w_inner, w_write, w_read, w_gate, w_pool_in], axis=1)
     projected = jnp.dot(
-        whole_rows,
-        lax.all_gather(stacked, SP, axis=0, tiled=True),
-        preferred_element_type=jnp.float32,
+        whole_rows, all_by_exchange(stacked, SP, 0), preferred_element_type=jnp.float32
     )
     projected = projected.astype(jnp.bfloat16)
     stream_cols = inner_here + 2 * cross_here

time: 370 us -> 519 us (1.40)
  waiting for transfers between devices: 163 us -> 253 us
  blocking collectives: 57.1 us -> 92.8 us
  starting transfers between devices: 21.7 us -> 45.7 us
    all_to_all x0 -> x1, waiting for transfers between devices: none -> 172 us  [all_by_exchange(): parts = lax.all_to_all(parts, axis, split_axis=0, concat_axis=0)]
    all_gather x1 -> x0, waiting for transfers between devices: 78.8 us -> none  [body(): lax.all_gather(stacked, SP, axis=0, tiled=True)]
    all_gather x4, blocking collectives: 51.3 us -> 87 us  [prefix_by_axis(): lax.all_gather(part.astype(kind), axis)]
    ppermute x2, starting transfers between devices: 8.68 us -> 21.3 us  [with_halo(): lax.ppermute(lax.slice_in_dim(block, block.shape[dim] - width, None, axis...]
    all_to_all x0 -> x1, starting transfers between devices: none -> 11.3 us  [all_by_exchange(): parts = lax.all_to_all(parts, axis, split_axis=0, concat_axis=0)]
  transfers between devices with their start and end apart: 11 -> 11, of which waited for: 7 -> 7; matrix products, arithmetic and copies ran while one was open for 24% -> 17% of each run, Pallas kernels for 0% -> 0%
where the time goes in v1:
time: 519 us; the launch traced here: 518 us
  waiting for transfers between devices  253 us (49%)
  blocking collectives  92.8 us (18%)
  local copies, waits for them, and re-layouts  61.4 us (12%)
  starting transfers between devices  45.7 us (9%)
  other arithmetic  32.1 us (6%)
  matrix products  18.1 us (3%)
  between operations  15 us (3%)
    all_to_all x1, waiting for transfers between devices, all_by_exchange(): parts = lax.all_to_all(parts, axis, split_axis=0, concat_axis=0)  172 us
    all_gather x4, blocking collectives, prefix_by_axis(): lax.all_gather(part.astype(kind), axis)  87 us
    all_gather x4, waiting for transfers between devices, prefix_by_axis(): lax.all_gather(part.astype(kind), axis)  47.9 us
    all_gather x1, waiting for transfers between devices, sent_together(): lax.all_gather(both, axis, axis=dim, tiled=True)  31.4 us
    ppermute x2, starting transfers between devices, with_halo(): lax.ppermute(lax.slice_in_dim(block, block.shape[dim] - width, None, axis...  21.3 us
    exp x30, local copies, waits for them, and re-layouts, merge_states(): jnp.exp(later[0])[:, None, None]  19.4 us
    all_to_all x1, starting transfers between devices, all_by_exchange(): parts = lax.all_to_all(parts, axis, split_axis=0, concat_axis=0)  11.3 us
  transfers between devices with their start and end apart: 11, of which 7 were waited for; matrix products, arithmetic and copies ran while one was open for 17% of the time, Pallas kernels for 0%

profile of v1, /device:TPU:1, one launch (start us, length us, event | category | flops | bytes accessed | tf_op | source)
XLA Modules:
  0.0 518.3 jit_solution(5871400976904105801)
XLA Ops:
  6.6 1.1 copy.59
  7.7 0.8 broadcast_in_dim.44
  8.5 10.3 %all-to-all-start.1 = ((bf16[2,256,512]{1,2,0:T(8,128)(2,1)}), bf16[2,256,512]{1,2,0:T(8,128)(2,1)S(1)}, u32[]{:S(2)}, u32[]{:S(2)}) async-start(bf16[2,256,512]{1,2,0:T(8,128)(2,1)} %broadcast_in_dim.44), calls=%async_computation.1 | async-start | bytes 1048576 | tf_op jit(solution)/shard_map/all_to_all | solution.py:50
  18.9 1.3 all-to-all-done.1
  20.2 3.4 stack.2
  23.7 11.3 %all-to-all-start = ((bf16[64,16,3072]{2,1,0:T(8,128)(2,1)}), bf16[64,16,3072]{2,1,0:T(8,128)(2,1)}, u32[]{:S(2)}, u32[]{:S(2)}) async-start(bf16[64,16,3072]{2,1,0:T(8,128)(2,1)} %stack.2), calls=%async_computation | async-start | bytes 12582912 | tf_op jit(solution)/shard_map/all_to_all | solution.py:22
  35.5 1.2 reduce_window_sum.67
  37.7 171.7 %all-to-all-done = bf16[64,16,3072]{2,1,0:T(8,128)(2,1)} async-done(((bf16[64,16,3072]{2,1,0:T(8,128)(2,1)}), bf16[64,16,3072]{2,1,0:T(8,128)(2,1)}, u32[]{:S(2)}, u32[]{:S(2)}) %all-to-all-start) | async-done | bytes 6291488 | tf_op jit(solution)/shard_map/all_to_all | solution.py:22
  209.4 4.6 fusion
  214.1 1.3 collective-permute-start.1
  215.4 16.6 %collective-permute-start = (bf16[2,1536]{1,0:T(2,128)(2,1)S(1)}, bf16[2,1536]{1,0:T(2,128)(2,1)S(1)}, u32[]{:S(2)}, u32[]{:S(2)}) collective-permute-start(bf16[2,1536]{1,0:T(2,128)(2,1)S(1)} %get-tuple-element.94), channel_id=1, source_target_pairs={{0,8},{8,16},{16,24},{24,32},{32,40},{40,48},{48,56},{56,64},{64,7... | collective-permute-start | bytes 18440 | tf_op jit(solution)/shard_map/ppermute | solution.py:31
  233.0 1.1 divide_multiply_fusion
  235.2 1.5 broadcast_multiply_fusion.2
  237.0 0.7 fusion.63
  237.7 0.7 convert_element_type.916
  238.7 1.2 reduce_window_sum.70
  240.9 1.3 rev.15
  242.2 1.7 reshape.1095
  245.0 0.7 fusion.60
  245.7 0.7 convert_element_type.986
  246.6 49.5 %all-gather = bf16[8,1,16]{2,1,0:T(2,128)(2,1)S(1)} all-gather(bf16[1,1,16]{2,1,0:T(2,128)(2,1)S(1)} %reshape.1184), channel_id=1, replica_groups=mesh['sp_0'=8,'sp_1'=8,'fs'=4,'tp'=2] {'sp_1'}, dimensions={0}, use_global_device_ids=true | all-gather | bytes 288 | tf_op jit(solution)/shard_map/all_gather | solution.py:78
  296.2 18.0 %all-gather.10.cloned.1.call-done = bf16[8,16,64,128]{3,2,1,0:T(8,128)(2,1)} async-done(((bf16[1,16,64,128]{3,2,1,0:T(8,128)(2,1)}), bf16[8,16,64,128]{3,2,1,0:T(8,128)(2,1)}) %all-gather.10.cloned.1.call-update) | async-done | bytes 2097168 | tf_op jit(solution)/shard_map/all_gather | solution.py:78
  314.2 2.7 add_convert_fusion.1
  317.2 11.3 %all-gather.2 = bf16[8,1,16]{2,1,0:T(2,128)(2,1)S(1)} all-gather(bf16[1,1,16]{2,1,0:T(2,128)(2,1)S(1)} %reshape.1188), channel_id=1, replica_groups=mesh['sp_0'=8,'sp_1'=8,'fs'=4,'tp'=2] {'sp_1'}, dimensions={0}, use_global_device_ids=true | all-gather | bytes 288 | tf_op jit(solution)/shard_map/all_gather | solution.py:78
  328.6 29.9 %all-gather.14.cloned.1.call-done = bf16[8,16,64,128]{3,2,1,0:T(8,128)(2,1)} async-done(((bf16[1,16,64,128]{3,2,1,0:T(8,128)(2,1)}), bf16[8,16,64,128]{3,2,1,0:T(8,128)(2,1)}) %all-gather.14.cloned.1.call-update) | async-done | bytes 2097168 | tf_op jit(solution)/shard_map/all_gather | solution.py:78
  358.5 2.7 add_convert_fusion
  361.4 1.0 pad_maximum_fusion
  371.4 13.8 %all-gather.3 = bf16[8,1,16]{2,1,0:T(2,128)(2,1)S(1)} all-gather(bf16[1,1,16]{2,1,0:T(2,128)(2,1)S(1)} %get-tuple-element.46), channel_id=1, replica_groups=mesh['sp_0'=8,'sp_1'=8,'fs'=4,'tp'=2] {'sp_0'}, dimensions={0}, use_global_device_ids=true | all-gather | bytes 288 | tf_op jit(solution)/shard_map/all_gather | solution.py:78
  385.2 12.3 %all-gather.1 = bf16[8,1,16]{2,1,0:T(2,128)(2,1)S(1)} all-gather(bf16[1,1,16]{2,1,0:T(2,128)(2,1)S(1)} %get-tuple-element.50), channel_id=1, replica_groups=mesh['sp_0'=8,'sp_1'=8,'fs'=4,'tp'=2] {'sp_0'}, dimensions={0}, use_global_device_ids=true | all-gather | bytes 288 | tf_op jit(solution)/shard_map/all_gather | solution.py:78
  403.3 0.7 copy.71
  415.1 0.7 copy.91
  418.5 1.3 convert_multiply_fusion
  419.8 1.0 slice.520
  420.8 1.3 collective-permute-start.3
  422.1 4.7 collective-permute-start.2
  427.2 0.9 fusion.106
  428.3 0.9 fusion.103
  429.4 2.5 maximum_convert_fusion.1
  431.8 2.3 reshape.1145
  436.8 0.9 fusion.37
  437.7 1.9 slice_convert_fusion.15
  439.6 0.8 copy-done.4
  440.4 1.9 slice_convert_fusion.7
  442.5 1.8 fusion.242
  445.0 1.3 fusion.79
  446.4 0.9 fusion.32
  447.7 0.7 copy-done.26
  448.5 0.9 fusion.22
  449.4 1.8 copy.77
  451.2 2.1 reshape.1093
  453.5 1.8 fusion.241
  456.0 1.3 fusion.68
  457.3 0.9 fusion.31
  458.6 0.9 copy-done.6
  459.5 0.9 fusion.28
  460.4 1.8 copy.94
  462.2 3.0 reshape.1100
  465.3 2.3 rev.19
  467.5 1.7 multiply_reduce_fusion
  469.6 31.4 %all-gather.18.cloned.1.call-done = bf16[1536,1024]{1,0:T(8,128)(2,1)} async-done(((bf16[1536,256]{1,0:T(8,128)(2,1)}), bf16[1536,1024]{1,0:T(8,128)(2,1)}) %all-gather.18.cloned.1.call-update) | async-done | bytes 3145744 | tf_op jit(solution)/shard_map/all_gather | solution.py:45
  501.0 2.4 fusion.1
  503.3 1.8 fusion.35
  505.1 5.8 %all_to_all.15 = bf16[2,128,1024]{2,1,0:T(8,128)(2,1)S(1)} all-to-all(bf16[2,128,1024]{2,1,0:T(8,128)(2,1)S(1)} %bitcast.453), channel_id=1, replica_groups=mesh['sp_0'=8,'sp_1'=8,'fs'=4,'tp'=2] {'tp'}, dimensions={0} | all-to-all | bytes 1048576 | tf_op jit(solution)/shard_map/all_to_all | solution.py:100
  510.9 0.8 reduce_sum.22
  (349 shorter events, 40.6 us)
Async XLA Ops:
  6.5 430.0 %copy-start = (bf16[4,256,256]{2,1,0:T(8,128)(2,1)S(1)}, bf16[4,256,256]{2,1,0:T(8,128)(2,1)}, u32[]{:S(2)}) copy-start(bf16[4,256,256]{2,1,0:T(8,128)(2,1)} %param.28) | copy-start | bytes 1572868
  6.5 12.3 %copy-start.47 = (bf16[16,1024]{1,0:T(8,128)(2,1)S(1)}, bf16[16,1024]{1,0:T(8,128)(2,1)}, u32[]{:S(2)}) copy-start(bf16[16,1024]{1,0:T(8,128)(2,1)} %param.17) | copy-start | bytes 98308
  6.5 12.3 %copy-start.60 = (bf16[16,256]{1,0:T(8,128)(2,1)S(1)}, bf16[16,256]{1,0:T(8,128)(2,1)}, u32[]{:S(2)}) copy-start(bf16[16,256]{1,0:T(8,128)(2,1)} %param.19) | copy-start | bytes 24580
  6.5 12.3 %copy-start.61 = (bf16[16,256]{1,0:T(8,128)(2,1)S(1)}, bf16[16,256]{1,0:T(8,128)(2,1)}, u32[]{:S(2)}) copy-start(bf16[16,256]{1,0:T(8,128)(2,1)} %param.20) | copy-start | bytes 24580
  6.5 12.3 %copy-start.48 = (bf16[16,1024]{1,0:T(8,128)(2,1)S(1)}, bf16[16,1024]{1,0:T(8,128)(2,1)}, u32[]{:S(2)}) copy-start(bf16[16,1024]{1,0:T(8,128)(2,1)} %param.18) | copy-start | bytes 98308
  6.5 12.4 %copy-start.50 = (bf16[16,512]{1,0:T(8,128)(2,1)S(1)}, bf16[16,512]{1,0:T(8,128)(2,1)}, u32[]{:S(2)}) copy-start(bf16[16,512]{1,0:T(8,128)(2,1)} %param.21) | copy-start | bytes 49156
  8.5 11.7 %all-to-all-start.1 = ((bf16[2,256,512]{1,2,0:T(8,128)(2,1)}), bf16[2,256,512]{1,2,0:T(8,128)(2,1)S(1)}, u32[]{:S(2)}, u32[]{:S(2)}) async-start(bf16[2,256,512]{1,2,0:T(8,128)(2,1)} %broadcast_in_dim.44), calls=%async_computation.1 | async-start | bytes 1048576 | tf_op jit(solution)/shard_map/all_to_all | solution.py:50
  23.6 11.4 %copy-start.99 = (f32[2,32]{1,0:T(2,128)S(1)}, f32[2,32]{1,0:T(2,128)}, u32[]{:S(2)}) copy-start(f32[2,32]{1,0:T(2,128)} %param.25) | copy-start | bytes 772
  23.6 11.5 %copy-start.46 = (bf16[1024,2,32]{0,2,1:T(8,128)(2,1)S(1)}, bf16[1024,2,32]{0,2,1:T(8,128)(2,1)}, u32[]{:S(2)}) copy-start(bf16[1024,2,32]{0,2,1:T(8,128)(2,1)} %param.22) | copy-start | bytes 393220
  23.6 11.7 %copy-start.49 = (f32[1,256,2,16]{1,3,2,0:T(8,128)S(1)}, f32[1,256,2,16]{1,3,2,0:T(8,128)}, u32[]{:S(2)}) copy-start(f32[1,256,2,16]{1,3,2,0:T(8,128)} %param.26) | copy-start | bytes 98308
  23.6 13.8 %copy-start.40 = (bf16[5,2,512]{2,1,0:T(2,128)(2,1)S(1)}, bf16[5,2,512]{2,1,0:T(2,128)(2,1)}, u32[]{:S(2)}) copy-start(bf16[5,2,512]{2,1,0:T(2,128)(2,1)} %param.24) | copy-start | bytes 30724
  23.6 14.0 %copy-start.59 = (bf16[5,2048]{1,0:T(8,128)(2,1)S(1)}, bf16[5,2048]{1,0:T(8,128)(2,1)}, u32[]{:S(2)}) copy-start(bf16[5,2048]{1,0:T(8,128)(2,1)} %param.23) | copy-start | bytes 61444
  23.7 185.7 %all-to-all-start = ((bf16[64,16,3072]{2,1,0:T(8,128)(2,1)}), bf16[64,16,3072]{2,1,0:T(8,128)(2,1)}, u32[]{:S(2)}, u32[]{:S(2)}) async-start(bf16[64,16,3072]{2,1,0:T(8,128)(2,1)} %stack.2), calls=%async_computation | async-start | bytes 12582912 | tf_op jit(solution)/shard_map/all_to_all | solution.py:22
  35.0 279.2 %all-gather.10.cloned.1.call-start = ((), (), s32[]{:S(2)}) async-start(), calls=%async_computation.3 | async-start | bytes 2359296 | tf_op jit(solution)/shard_map/all_gather | solution.py:78
  36.8 177.3 %copy-start.42 = (f32[2,2,8]{2,1,0:T(2,128)}, f32[2,2,8]{2,1,0:T(2,128)S(1)}, u32[]{:S(2)}) copy-start(f32[2,2,8]{2,1,0:T(2,128)S(1)} %slice_reduce_fusion.1) | copy-start | bytes 388
  37.5 208.9 %copy-start.36 = (f32[2,2,8]{2,1,0:T(2,128)}, f32[2,2,8]{2,1,0:T(2,128)S(1)}, u32[]{:S(2)}) copy-start(f32[2,2,8]{2,1,0:T(2,128)S(1)} %fusion.249) | copy-start | bytes 388
  214.0 18.9 %copy-start.19 = (bf16[256,3072]{1,0:T(8,128)(2,1)}, bf16[256,3072]{1,0:T(8,128)(2,1)S(1)}, u32[]{:S(2)}) copy-start(bf16[256,3072]{1,0:T(8,128)(2,1)S(1)} %fusion) | copy-start | bytes 4718596
  214.1 18.0 %collective-permute-start.1 = (bf16[2,1536]{1,0:T(2,128)(2,1)S(1)}, bf16[2,1536]{1,0:T(2,128)(2,1)S(1)}, u32[]{:S(2)}, u32[]{:S(2)}) collective-permute-start(bf16[2,1536]{1,0:T(2,128)(2,1)S(1)} %get-tuple-element.95), channel_id=1, source_target_pairs={{8,0},{16,8},{24,16},{32,24},{40,32},{48,40},{56,48},{64,56},{72,6... | collective-permute-start | bytes 18440 | tf_op jit(solution)/shard_map/ppermute | solution.py:34
  215.4 17.3 %collective-permute-start = (bf16[2,1536]{1,0:T(2,128)(2,1)S(1)}, bf16[2,1536]{1,0:T(2,128)(2,1)S(1)}, u32[]{:S(2)}, u32[]{:S(2)}) collective-permute-start(bf16[2,1536]{1,0:T(2,128)(2,1)S(1)} %get-tuple-element.94), channel_id=1, source_target_pairs={{0,8},{8,16},{16,24},{24,32},{32,40},{40,48},{48,56},{56,64},{64,7... | collective-permute-start | bytes 18440 | tf_op jit(solution)/shard_map/ppermute | solution.py:31
  236.9 3.7 copy-start.24
  238.4 120.1 %all-gather.14.cloned.1.call-start = ((), (), s32[]{:S(2)}) async-start(), calls=%async_computation.5 | async-start | bytes 2359296 | tf_op jit(solution)/shard_map/all_gather | solution.py:78
  239.8 2.4 copy-start.30
  240.0 2.2 copy-start.44
  245.0 72.0 %copy-start.22 = (bf16[2,2,8,64,128]{4,3,2,1,0:T(8,128)(2,1)}, bf16[2,2,8,64,128]{4,3,2,1,0:T(8,128)(2,1)S(1)}, u32[]{:S(2)}) copy-start(bf16[2,2,8,64,128]{4,3,2,1,0:T(8,128)(2,1)S(1)} %fusion.43) | copy-start | bytes 1572868
  246.4 70.6 %copy-start.39 = (f32[2,2,8]{2,1,0:T(2,128)S(1)}, f32[2,2,8]{2,1,0:T(2,128)}, u32[]{:S(2)}) copy-start(f32[2,2,8]{2,1,0:T(2,128)} %copy-done.38) | copy-start | bytes 388
  246.4 195.9 %all-gather.12.cloned.1.call-start = ((), (), s32[]{:S(2)}) async-start(), calls=%async_computation.4 | async-start | bytes 2359296 | tf_op jit(solution)/shard_map/all_gather | solution.py:78
  316.9 44.4 %copy-start.20 = (bf16[1024,256]{1,0:T(8,128)(2,1)S(1)}, bf16[1024,256]{1,0:T(8,128)(2,1)}, u32[]{:S(2)}) copy-start(bf16[1024,256]{1,0:T(8,128)(2,1)} %param.30) | copy-start | bytes 1572868
  316.9 44.4 %copy-start.29 = (bf16[512,256]{1,0:T(8,128)(2,1)S(1)}, bf16[512,256]{1,0:T(8,128)(2,1)}, u32[]{:S(2)}) copy-start(bf16[512,256]{1,0:T(8,128)(2,1)} %param.31) | copy-start | bytes 786436
  317.0 136.5 %all-gather.16.cloned.1.call-start = ((), (), s32[]{:S(2)}) async-start(), calls=%async_computation.6 | async-start | bytes 2359296 | tf_op jit(solution)/shard_map/all_gather | solution.py:78
  361.2 3.0 copy-start.45
  361.2 3.7 dynamic-slice-start
  361.2 55.2 %copy-start.98 = (f32[1024]{0:T(1024)S(1)}, f32[1024]{0:T(1024)}, u32[]{:S(2)}) copy-start(f32[1024]{0:T(1024)} %param.29) | copy-start | bytes 12292
  361.3 139.7 %all-gather.18.cloned.1.call-start = ((), (), s32[]{:S(2)}) async-start(), calls=%async_computation.7 | async-start | bytes 3932160 | tf_op jit(solution)/shard_map/all_gather | solution.py:45
  420.8 8.4 %collective-permute-start.3 = (bf16[256,512]{1,0:T(8,128)(2,1)S(1)}, bf16[256,512]{1,0:T(8,128)(2,1)}, u32[]{:S(2)}, u32[]{:S(2)}) collective-permute-start(bf16[256,512]{1,0:T(8,128)(2,1)S(1)} %slice.520), channel_id=1, source_target_pairs={{8,0},{16,8},{24,16},{32,24},{40,32},{48,40},{56,48},{64,56},{72,6... | collective-permute-start | bytes 786440 | tf_op jit(solution)/shard_map/ppermute | solution.py:34
  422.1 7.3 %collective-permute-start.2 = (bf16[256,512]{1,0:T(8,128)(2,1)S(1)}, bf16[256,512]{1,0:T(8,128)(2,1)}, u32[]{:S(2)}, u32[]{:S(2)}) collective-permute-start(bf16[256,512]{1,0:T(8,128)(2,1)S(1)} %slice.520), channel_id=1, source_target_pairs={{0,8},{8,16},{16,24},{24,32},{32,40},{40,48},{48,56},{56,64},{64,7... | collective-permute-start | bytes 786440 | tf_op jit(solution)/shard_map/ppermute | solution.py:31
  437.7 2.7 copy-start.4
  442.3 2.2 copy-start.16
  442.4 2.3 copy-start.17
  442.4 2.5 copy-start.18
  442.4 2.5 copy-start.81
  442.4 2.5 copy-start.82
  442.4 2.5 copy-start.83
  442.4 2.5 copy-start.84
  442.4 2.5 copy-start.85
  442.4 2.5 copy-start.86
  442.4 2.5 copy-start.87
  442.4 2.5 copy-start.88
  442.4 2.5 copy-start.89
  442.5 2.5 copy-start.90
  442.5 2.5 copy-start.91
  442.5 2.5 copy-start.92
  442.5 2.5 copy-start.93
  442.5 2.5 copy-start.94
  442.5 2.5 copy-start.95
  442.5 2.5 copy-start.96
  442.5 2.5 copy-start.97
  453.3 2.1 copy-start.64
  453.3 2.1 copy-start.65
  453.3 2.1 copy-start.66
  453.5 2.1 copy-start.10
  453.5 2.3 copy-start.11
  453.5 2.4 copy-start.12
  501.0 2.4 copy-start.21
  503.3 8.4 %copy-start.1 = (bf16[4,256,256]{2,1,0:T(8,128)(2,1)S(1)}, bf16[4,256,256]{2,1,0:T(8,128)(2,1)}, u32[]{:S(2)}) copy-start(bf16[4,256,256]{2,1,0:T(8,128)(2,1)} %param.28) | copy-start | bytes 1572868
  (50 other events, 79.4 us)
Sparse Core Ops, SparseCore 0:
  238.5 75.6 all-gather.9
  316.3 42.1 all-gather.13
  360.6 42.7 all-gather.11
  405.3 46.8 all-gather.15
  454.1 46.7 all-gather.17
